TPU v7x, 32 devices: a whole 2x2x4 slice. The times are simulated.
32 devices in a mesh: sp: 8 (over z, x), tp: 4 (over y, core).
Axes of the slice: x: 2, y: 2, z: 4, core: 2. Of those that a mesh axis runs over, the one named last changes fastest.
Arguments:
- tokens: bfloat16 [2048, 2048], P('sp', 'tp'), may hold values from -6 to 6
- norm_gain: float32 [2048], replicated, may hold values from 0.1 to 1.9
- query_one: bfloat16 [2048, 512], P('sp', 'tp'), may hold values from -1 to 1
- key_one: bfloat16 [2048, 512], P('sp', 'tp'), may hold values from -1 to 1
- query_two: bfloat16 [2048, 512], P('sp', 'tp'), may hold values from -0.15625 to 0.15625
- key_two: bfloat16 [2048, 512], P('sp', 'tp'), may hold values from -0.15625 to 0.15625
- value_weight: bfloat16 [2048, 1024], P('sp', 'tp'), may hold values from -0.5 to 0.5
- pool_weight: bfloat16 [2048, 1024], P('sp', 'tp'), may hold values from -0.125 to 0.125
- lambda_head: float32 [8], replicated, may hold values from 0.3 to 0.8
- head_gain: float32 [128], replicated, may hold values from 0.1 to 1.9
- group_weight: bfloat16 [8, 128, 128], replicated, may hold values from -0.5 to 0.5
- pool_scale: float32 [1024], replicated, may hold values from 0.1 to 1.9
- out_attn: bfloat16 [1024, 2048], P('tp', 'sp'), may hold values from -0.125 to 0.125
- out_pool: bfloat16 [1024, 2048], P('tp', 'sp'), may hold values from -0.125 to 0.125
Outputs:
- mixed: bfloat16 [2048, 2048], P(('sp', 'tp'))
All inputs are finite; a program needn't handle non-finite values.
Results may differ from a plain program's by a relative error of at most 0.013.
Values may be sent and summed in bfloat16 or wider, within the bound.
A program may use at most 128 MiB of HBM per device.

v0:
```python
import math
import jax
import jax.numpy as jnp
from jax import lax
from jax.sharding import PartitionSpec as P

HEAD_DIM = 64
VALUE_DIM = 128
GROUP_DIM = 128
rope_base = 500000.0
head_scale = 0.8
norm_floor = 1e-06
head_floor = 0.001
masked_score = -1e30
pool_reach = 15
key_block = 1024


def from_behind(x, axis, by):
    peers = lax.axis_size(axis)
    pairs = [(i, i + by) for i in range(peers) if 0 <= i + by < peers]
    return lax.ppermute(x, axis, pairs)


def rotate(values_in, positions):
    half_dim = values_in.shape[-1] // 2
    inverse = rope_base ** (-(jnp.arange(half_dim, dtype=jnp.float32) * 2.0 / values_in.shape[-1]))
    angles = positions.astype(jnp.float32)[:, None] * inverse[None, :]
    cosine = jnp.cos(angles)[:, None, :]
    sine_part = jnp.sin(angles)[:, None, :]
    first_half = values_in[..., :half_dim]
    second_half = values_in[..., half_dim:]
    return jnp.concatenate(
        [
            first_half * cosine - second_half * sine_part,
            second_half * cosine + first_half * sine_part,
        ],
        axis=-1,
    )


def body(
    tokens,
    norm_gain,
    query_one,
    key_one,
    query_two,
    key_two,
    value_weight,
    pool_weight,
    lambda_head,
    head_gain,
    group_weight,
    pool_scale,
    out_attn,
    out_pool,
):
    tok_rows = tokens.shape[0]
    local_heads = query_one.shape[1] // HEAD_DIM
    local_groups = pool_weight.shape[1] // GROUP_DIM
    tp_index = lax.axis_index("tp")
    positions = lax.axis_index("sp") * tok_rows + jnp.arange(tok_rows, dtype=jnp.int32)
    score_scale = HEAD_DIM ** (-0.5)
    gathered = lax.all_gather(tokens, "tp", axis=1, tiled=True)
    float_rows = gathered.astype(jnp.float32)
    normed = (
        float_rows
        * lax.rsqrt(jnp.mean(float_rows * float_rows, axis=-1, keepdims=True) + norm_floor)
        * norm_gain
    ).astype(jnp.bfloat16)

    def contract(shard_part):
        return jnp.dot(normed, shard_part, preferred_element_type=jnp.float32)

    pieces = (
        lax.all_gather(query_one, "sp", axis=0, tiled=True),
        lax.all_gather(key_one, "sp", axis=0, tiled=True),
        lax.all_gather(query_two, "sp", axis=0, tiled=True),
        lax.all_gather(key_two, "sp", axis=0, tiled=True),
        lax.all_gather(value_weight, "sp", axis=0, tiled=True),
    )
    projected = tuple((contract(shard_part) for shard_part in pieces))
    pool_proj = contract(lax.all_gather(pool_weight, "sp", axis=0, tiled=True))

    def turned(flat_part):
        return rotate(flat_part.reshape(tok_rows, local_heads, HEAD_DIM), positions).astype(
            jnp.bfloat16
        )

    query_a = turned(projected[0])
    key_a = turned(projected[1]).reshape(tok_rows, local_heads * HEAD_DIM)
    query_b = turned(projected[2])
    key_b = turned(projected[3]).reshape(tok_rows, local_heads * HEAD_DIM)
    value_rows = projected[4].astype(jnp.bfloat16)
    queries = (query_a, query_b)
    initial = (
        jnp.full((2, tok_rows, local_heads), masked_score, jnp.float32),
        jnp.zeros((2, tok_rows, local_heads), jnp.float32),
        jnp.zeros((2, tok_rows, local_heads, VALUE_DIM), jnp.float32),
    )
    pieces = (
        lax.all_gather(key_a, "sp", axis=0, tiled=True),
        lax.all_gather(key_b, "sp", axis=0, tiled=True),
        lax.all_gather(value_rows, "sp", axis=0, tiled=True),
    )
    key_rows = pieces[0].shape[0]
    key_span = math.gcd(key_rows, key_block)
    count_blocks = key_rows // key_span
    stacked = tuple((member.reshape(count_blocks, key_span, local_heads, -1) for member in pieces))

    def step_block(carried, inputs):
        maxima, totals, accums = carried
        block_a, block_b, block_v, block_id = inputs
        key_pos = block_id * key_span + jnp.arange(key_span, dtype=jnp.int32)
        visible = (key_pos[None, :] <= positions[:, None])[:, None, :]
        new_maxima, new_totals, new_accums = ([], [], [])
        for map_index, key_part in enumerate((block_a, block_b)):
            scores = (
                jnp.einsum(
                    "qhd,khd->qhk", queries[map_index], key_part, preferred_element_type=jnp.float32
                )
                * score_scale
            )
            scores = jnp.where(visible, scores, masked_score)
            top_now = jnp.maximum(maxima[map_index], jnp.max(scores, axis=-1))
            factor = jnp.exp(maxima[map_index] - top_now)
            weights = jnp.where(visible, jnp.exp(scores - top_now[..., None]), 0.0)
            new_maxima.append(top_now)
            new_totals.append(totals[map_index] * factor + jnp.sum(weights, axis=-1))
            product = jnp.einsum(
                "qhk,khd->qhd",
                weights.astype(jnp.bfloat16),
                block_v,
                preferred_element_type=jnp.float32,
            )
            new_accums.append(accums[map_index] * factor[..., None] + product)
        return ((jnp.stack(new_maxima), jnp.stack(new_totals), jnp.stack(new_accums)), None)

    result_state, _ = lax.scan(
        step_block,
        initial,
        (stacked[0], stacked[1], stacked[2], jnp.arange(count_blocks, dtype=jnp.int32)),
    )
    maxima, totals, accums = result_state
    map_means = accums / totals[..., None]
    lambda_local = lax.dynamic_slice_in_dim(lambda_head, tp_index * local_heads, local_heads, 0)
    differed = map_means[0] - lambda_local[None, :, None] * map_means[1]
    scaled = (
        differed
        * lax.rsqrt(jnp.mean(differed * differed, axis=-1, keepdims=True) + head_floor)
        * head_gain
        * head_scale
    )
    attn_out = scaled.reshape(tok_rows, local_heads * VALUE_DIM).astype(jnp.bfloat16)
    pool_rows = pool_proj.astype(jnp.bfloat16)
    prior_rows = from_behind(pool_rows[tok_rows - pool_reach :], "sp", 1)
    extended = jnp.concatenate([prior_rows, pool_rows], axis=0).astype(jnp.float32)
    group_ids = tp_index * local_groups + jnp.arange(local_groups, dtype=jnp.int32)
    windows = jnp.left_shift(2, group_ids % 4)
    channel_windows = (windows[:, None] + jnp.zeros((1, GROUP_DIM), jnp.int32)).reshape(-1)
    window_sum = jnp.zeros((tok_rows, local_groups * GROUP_DIM), jnp.float32)
    for lag_steps in range(pool_reach + 1):
        keep_mask = (lag_steps < channel_windows).astype(jnp.float32)
        window_sum = (
            window_sum
            + extended[pool_reach - lag_steps : pool_reach - lag_steps + tok_rows]
            * keep_mask[None, :]
        )
    counts = jnp.minimum(positions[:, None] + 1, channel_windows[None, :]).astype(jnp.float32)
    window_mean = window_sum / counts - pool_rows.astype(jnp.float32)
    local_mixing = lax.dynamic_slice_in_dim(group_weight, tp_index * local_groups, local_groups, 0)
    grouped = jnp.einsum(
        "tgc,gcd->tgd",
        window_mean.astype(jnp.bfloat16).reshape(tok_rows, local_groups, GROUP_DIM),
        local_mixing,
        preferred_element_type=jnp.float32,
    )
    scale_local = lax.dynamic_slice_in_dim(
        pool_scale, tp_index * local_groups * GROUP_DIM, local_groups * GROUP_DIM, 0
    )
    pooled = (grouped.reshape(tok_rows, local_groups * GROUP_DIM) * scale_local).astype(
        jnp.bfloat16
    )
    attn_cols, pool_cols = (
        lax.all_gather(out_attn, "sp", axis=1, tiled=True),
        lax.all_gather(out_pool, "sp", axis=1, tiled=True),
    )
    return lax.psum_scatter(
        (
            jnp.dot(attn_out, attn_cols, preferred_element_type=jnp.float32)
            + jnp.dot(pooled, pool_cols, preferred_element_type=jnp.float32)
        ).astype(jnp.bfloat16),
        "tp",
        scatter_dimension=0,
        tiled=True,
    )


def solution(mesh):
    in_specs = (
        P("sp", "tp"),
        P(),
        P("sp", "tp"),
        P("sp", "tp"),
        P("sp", "tp"),
        P("sp", "tp"),
        P("sp", "tp"),
        P("sp", "tp"),
        P(),
        P(),
        P(),
        P(),
        P("tp", "sp"),
        P("tp", "sp"),
    )
    out_specs = P(("sp", "tp"), None)
    return jax.shard_map(body, mesh=mesh, in_specs=in_specs, out_specs=out_specs, check_vma=False)
```

profile of v0, /device:TPU:0, one launch (start us, length us, event | category | flops | bytes accessed | tf_op | source)
XLA Modules:
  0.0 335.7 jit_solution(8059476277659263844)
XLA Ops:
  8.8 19.6 %all-gather.7.cloned.1.call-done = bf16[256,2048]{1,0:T(8,128)(2,1)} async-done(((bf16[256,512]{1,0:T(8,128)(2,1)}), bf16[256,2048]{1,0:T(8,128)(2,1)}) %all-gather.7.cloned.1.call-update) | async-done | bytes 1048592 | tf_op jit(solution)/shard_map/all_gather | solution.py:64
  28.4 1.5 fusion.41
  29.9 1.6 fusion.43
  31.5 39.3 %all-gather.9.cloned.1.call-done = bf16[2048,256]{1,0:T(8,128)(2,1)} async-done(((bf16[256,256]{1,0:T(8,128)(2,1)}), bf16[2048,256]{1,0:T(8,128)(2,1)}) %all-gather.9.cloned.1.call-update) | async-done | bytes 1048592 | tf_op jit(solution)/shard_map/all_gather | solution.py:80
  70.8 2.3 convolution_convert_fusion.1
  75.6 31.9 %all_gather.37 = bf16[2048,128]{1,0:T(8,128)(2,1)S(1)} all-gather(bf16[256,128]{1,0:T(8,128)(2,1)S(1)} %copy-done.4), channel_id=1, replica_groups=mesh['sp'=8,'tp'=4] {'sp'}, dimensions={0}, use_global_device_ids=true | all-gather | bytes 589824 | tf_op jit(solution)/shard_map/all_gather | solution.py:77
  107.5 32.2 %all_gather.39 = bf16[2048,128]{1,0:T(8,128)(2,1)S(1)} all-gather(bf16[256,128]{1,0:T(8,128)(2,1)S(1)} %copy-done.5), channel_id=1, replica_groups=mesh['sp'=8,'tp'=4] {'sp'}, dimensions={0}, use_global_device_ids=true | all-gather | bytes 589824 | tf_op jit(solution)/shard_map/all_gather | solution.py:76
  139.7 32.3 %all_gather.40 = bf16[2048,128]{1,0:T(8,128)(2,1)S(1)} all-gather(bf16[256,128]{1,0:T(8,128)(2,1)S(1)} %copy-done.6), channel_id=1, replica_groups=mesh['sp'=8,'tp'=4] {'sp'}, dimensions={0}, use_global_device_ids=true | all-gather | bytes 589824 | tf_op jit(solution)/shard_map/all_gather | solution.py:79
  172.0 31.9 %all_gather.42 = bf16[2048,128]{1,0:T(8,128)(2,1)S(1)} all-gather(bf16[256,128]{1,0:T(8,128)(2,1)S(1)} %copy-done.7), channel_id=1, replica_groups=mesh['sp'=8,'tp'=4] {'sp'}, dimensions={0}, use_global_device_ids=true | all-gather | bytes 589824 | tf_op jit(solution)/shard_map/all_gather | solution.py:78
  207.8 32.2 %all_gather.41 = bf16[2048,128]{0,1:T(8,128)(2,1)S(1)} all-gather(bf16[256,128]{0,1:T(8,128)(2,1)S(1)} %bitcast.251), channel_id=1, replica_groups=mesh['sp'=8,'tp'=4] {'sp'}, dimensions={0}, use_global_device_ids=true | all-gather | bytes 589824 | tf_op jit(solution)/shard_map/all_gather | solution.py:103
  240.0 31.2 %all_gather.38 = bf16[2048,128]{0,1:T(8,128)(2,1)S(1)} all-gather(bf16[256,128]{0,1:T(8,128)(2,1)S(1)} %bitcast.252), channel_id=1, replica_groups=mesh['sp'=8,'tp'=4] {'sp'}, dimensions={0}, use_global_device_ids=true | all-gather | bytes 589824 | tf_op jit(solution)/shard_map/all_gather | solution.py:102
  271.1 1.7 convolution_convert_fusion
  272.8 1.5 collective-permute-start
  277.1 1.3 reshape.313
  278.5 18.7 %while.15 = (s32[]{:T(128)}, f32[2,256,2]{1,2,0:T(2,128)S(1)}, f32[2,256,2]{1,2,0:T(2,128)S(1)}, f32[2,256,2,128]{1,3,2,0:T(8,128)S(1)}, s32[2]{0:T(128)S(1)}, /...) while((s32[]{:T(128)}, f32[2,256,2]{1,2,0:T(2,128)S(1)}, ...), condition=%wide.region_6.7_spmd.clone, body=%wide.region_1.6_spmd.clone.sunk | while | flops 416947456 | bytes 34822424 | solution.py:139
  280.1 1.8 fusion.141
  282.8 2.4 fusion.147
  285.2 1.0 fusion.143
  289.5 1.8 fusion.141
  292.1 2.4 fusion.147
  294.5 1.0 fusion.143
  297.6 1.7 fusion.101
  299.4 2.7 fusion.40
  302.1 26.7 %reduce-scatter.2.cloned.1.call-done = bf16[64,2048]{1,0:T(8,128)(2,1)} async-done(((bf16[256,2048]{1,0:T(8,128)(2,1)}), bf16[64,2048]{1,0:T(8,128)(2,1)}) %reduce-scatter.2.cloned.1.call-update) | async-done | bytes 262160 | tf_op jit(solution)/shard_map/reduce_scatter | solution.py:188
  (113 shorter events, 18.4 us)
Async XLA Ops:
  6.5 269.7 %copy-start = (bf16[8,128,128]{2,1,0:T(8,128)(2,1)S(1)}, bf16[8,128,128]{2,1,0:T(8,128)(2,1)}, u32[]{:S(2)}) copy-start(bf16[8,128,128]{2,1,0:T(8,128)(2,1)} %param.26) | copy-start | bytes 786436
  6.5 21.8 %all-gather.7.cloned.1.call-start = ((), (), s32[]{:S(2)}) async-start(), calls=%async_computation.1 | async-start | bytes 1310720 | tf_op jit(solution)/shard_map/all_gather | solution.py:64
  7.3 63.5 %all-gather.9.cloned.1.call-start = ((), (), s32[]{:S(2)}) async-start(), calls=%async_computation.2 | async-start | bytes 1179648 | tf_op jit(solution)/shard_map/all_gather | solution.py:80
  8.0 263.1 %all-gather.15.cloned.1.call-start = ((), (), s32[]{:S(2)}) async-start(), calls=%async_computation.5 | async-start | bytes 1179648 | tf_op jit(solution)/shard_map/all_gather | solution.py:83
  8.7 268.4 %all-gather.11.cloned.1.call-start = ((), (), s32[]{:S(2)}) async-start(), calls=%async_computation.3 | async-start | bytes 1179648 | tf_op jit(solution)/shard_map/all_gather | solution.py:104
  29.9 45.7 %copy-start.4 = (bf16[256,128]{1,0:T(8,128)(2,1)S(1)}, bf16[256,128]{1,0:T(8,128)(2,1)}, u32[]{:S(2)}) copy-start(bf16[256,128]{1,0:T(8,128)(2,1)} %param.19) | copy-start | bytes 196612
  31.5 76.1 %copy-start.5 = (bf16[256,128]{1,0:T(8,128)(2,1)S(1)}, bf16[256,128]{1,0:T(8,128)(2,1)}, u32[]{:S(2)}) copy-start(bf16[256,128]{1,0:T(8,128)(2,1)} %param.18) | copy-start | bytes 196612
  31.5 108.2 %copy-start.6 = (bf16[256,128]{1,0:T(8,128)(2,1)S(1)}, bf16[256,128]{1,0:T(8,128)(2,1)}, u32[]{:S(2)}) copy-start(bf16[256,128]{1,0:T(8,128)(2,1)} %param.21) | copy-start | bytes 196612
  31.5 140.5 %copy-start.7 = (bf16[256,128]{1,0:T(8,128)(2,1)S(1)}, bf16[256,128]{1,0:T(8,128)(2,1)}, u32[]{:S(2)}) copy-start(bf16[256,128]{1,0:T(8,128)(2,1)} %param.20) | copy-start | bytes 196612
  31.5 173.4 %copy-start.8 = (f32[128]{0:T(128)S(1)}, f32[128]{0:T(128)}, u32[]{:S(2)}) copy-start(f32[128]{0:T(128)} %param.25) | copy-start | bytes 1540
  73.1 224.5 %all-gather.13.cloned.1.call-start = ((), (), s32[]{:S(2)}) async-start(), calls=%async_computation.4 | async-start | bytes 1179648 | tf_op jit(solution)/shard_map/all_gather | solution.py:185
  73.7 225.6 %all-gather.17.cloned.1.call-start = ((), (), s32[]{:S(2)}) async-start(), calls=%async_computation.6 | async-start | bytes 1179648 | tf_op jit(solution)/shard_map/all_gather | solution.py:186
  74.3 254.5 %reduce-scatter.2.cloned.1.call-start = ((), (), s32[]{:S(2)}) async-start(), calls=%async_computation.7 | async-start | bytes 1310720 | tf_op jit(solution)/shard_map/reduce_scatter | solution.py:188
  272.8 3.3 collective-permute-start
  274.3 1.9 copy-start.10
  274.3 1.9 copy-start.11
  278.5 3.4 %copy-start.2 = (bf16[2,1024,2,64]{1,3,2,0:T(8,128)(2,1)}, bf16[2,1024,2,64]{1,3,2,0:T(8,128)(2,1)S(1)}, u32[]{:S(2)}) copy-start(bf16[2,1024,2,64]{1,3,2,0:T(8,128)(2,1)S(1)} %get-tuple-element.317) | copy-start | bytes 1572868 | tf_op jit(solution)/shard_map/while
  282.8 2.4 copy-start.1
  282.8 2.4 copy-start.9
  286.9 1.0 copy-start.3
  287.9 3.4 %copy-start.2 = (bf16[2,1024,2,64]{1,3,2,0:T(8,128)(2,1)}, bf16[2,1024,2,64]{1,3,2,0:T(8,128)(2,1)S(1)}, u32[]{:S(2)}) copy-start(bf16[2,1024,2,64]{1,3,2,0:T(8,128)(2,1)S(1)} %get-tuple-element.317) | copy-start | bytes 1572868 | tf_op jit(solution)/shard_map/while
  292.1 2.4 copy-start.1
  292.1 2.4 copy-start.9
  296.2 1.0 copy-start.3
Sparse Core Ops, SparseCore 0:
  8.9 19.4 all-gather.6
  30.5 40.2 all-gather.8
  72.9 41.6 all-gather.14
  116.6 41.4 all-gather.10
  160.0 42.5 all-gather.12
  204.4 40.6 all-gather.16
  302.2 26.5 reduce-scatter.1
where the time goes:
time: 336 us
  blocking collectives  192 us (57%)
  waiting for transfers between devices  88.8 us (26%)
  matrix products  22.8 us (7%)
  between operations  13.8 us (4%)
  local copies, waits for them, and re-layouts  9.14 us (3%)
  other arithmetic  6.18 us (2%)
    all_gather x1, waiting for transfers between devices, body(): lax.all_gather(value_weight, 'sp', axis=0, tiled=True)  39.3 us
    all_gather x1, blocking collectives, body(): lax.all_gather(key_two, 'sp', axis=0, tiled=True)  32.3 us
    all_gather x1, blocking collectives, body(): lax.all_gather(key_b, 'sp', axis=0, tiled=True)  32.2 us
    all_gather x1, blocking collectives, body(): lax.all_gather(query_one, 'sp', axis=0, tiled=True)  32.2 us
    all_gather x1, blocking collectives, body(): lax.all_gather(query_two, 'sp', axis=0, tiled=True)  31.9 us
    all_gather x1, blocking collectives, body(): lax.all_gather(key_one, 'sp', axis=0, tiled=True)  31.9 us
    all_gather x1, blocking collectives, body(): lax.all_gather(key_a, 'sp', axis=0, tiled=True)  31.2 us
    reduce_scatter x1, waiting for transfers between devices, body(): lax.psum_scatter((jnp.dot(attn_out, attn_cols, preferred_element_type=jnp...  26.7 us
  transfers between devices with their start and end apart: 8, of which 3 were waited for; matrix products, arithmetic and copies ran while one was open for 10% of the time, Pallas kernels for 0%

commit v1 on v0

--- a/solution.py
+++ b/solution.py
@@ -61,7 +61,12 @@
     tp_index = lax.axis_index("tp")
     positions = lax.axis_index("sp") * tok_rows + jnp.arange(tok_rows, dtype=jnp.int32)
     score_scale = HEAD_DIM ** (-0.5)
-    gathered = lax.all_gather(tokens, "tp", axis=1, tiled=True)
+    ring = [tokens]
+    for hop in range(3):
+        ring.append(lax.ppermute(ring[-1], "tp", [(dev, (dev + 1) % 4) for dev in range(4)]))
+    gathered = jnp.roll(
+        jnp.concatenate(ring[::-1], axis=1), (lax.axis_index("tp") + 1) * ring[0].shape[1], axis=1
+    )
     float_rows = gathered.astype(jnp.float32)
     normed = (
         float_rows

time: 336 us -> 316 us (0.940)
  waiting for transfers between devices: 88.8 us -> 69.9 us
    all_gather x1 -> x0, waiting for transfers between devices: 19.6 us -> none  [body(): gathered = lax.all_gather(tokens, 'tp', axis=1, tiled=True)]
    ppermute x0 -> x3, waiting for transfers between devices: none -> 17.7 us  [body(): lax.ppermute(ring[-1], 'tp', [(dev, (dev + 1) % 4) for dev in range(4)])]
    all_gather x1, waiting for transfers between devices: 39.3 us -> 24.9 us  [body(): lax.all_gather(value_weight, 'sp', axis=0, tiled=True)]
  transfers between devices with their start and end apart: 8 -> 10, of which waited for: 3 -> 5; matrix products, arithmetic and copies ran while one was open for 10% -> 10% of each run, Pallas kernels for 0% -> 0%
where the time goes in v1:
time: 316 us; the launch traced here: 315 us
  blocking collectives  192 us (61%)
  waiting for transfers between devices  69.9 us (22%)
  matrix products  22.7 us (7%)
  between operations  13.9 us (4%)
  local copies, waits for them, and re-layouts  9.66 us (3%)
  other arithmetic  3.75 us (1%)
    all_gather x1, blocking collectives, body(): lax.all_gather(query_two, 'sp', axis=0, tiled=True)  32.3 us
    all_gather x1, blocking collectives, body(): lax.all_gather(key_b, 'sp', axis=0, tiled=True)  32 us
    all_gather x1, blocking collectives, body(): lax.all_gather(key_two, 'sp', axis=0, tiled=True)  32 us
    all_gather x1, blocking collectives, body(): lax.all_gather(query_one, 'sp', axis=0, tiled=True)  31.9 us
    all_gather x1, blocking collectives, body(): lax.all_gather(key_one, 'sp', axis=0, tiled=True)  31.9 us
    all_gather x1, blocking collectives, body(): lax.all_gather(key_a, 'sp', axis=0, tiled=True)  31.5 us
    reduce_scatter x1, waiting for transfers between devices, body(): lax.psum_scatter((jnp.dot(attn_out, attn_cols, preferred_element_type=jnp...  25.4 us
    all_gather x1, waiting for transfers between devices, body(): lax.all_gather(value_weight, 'sp', axis=0, tiled=True)  24.9 us
  transfers between devices with their start and end apart: 10, of which 5 were waited for; matrix products, arithmetic and copies ran while one was open for 10% of the time, Pallas kernels for 0%

profile of v1, /device:TPU:0, one launch (start us, length us, event | category | flops | bytes accessed | tf_op | source)
XLA Modules:
  0.0 315.5 jit_solution(10207614538005891785)
XLA Ops:
  7.9 6.2 %collective-permute-done = bf16[256,512]{1,0:T(8,128)(2,1)S(1)} collective-permute-done((bf16[256,512]{1,0:T(8,128)(2,1)}, bf16[256,512]{1,0:T(8,128)(2,1)S(1)}, u32[]{:S(2)}, u32[]{:S(2)}) %collective-permute-start) | collective-permute-done | bytes 262176 | tf_op jit(solution)/shard_map/ppermute | solution.py:66
  14.1 5.8 %collective-permute-done.1 = bf16[256,512]{1,0:T(8,128)(2,1)S(1)} collective-permute-done((bf16[256,512]{1,0:T(8,128)(2,1)S(1)}, bf16[256,512]{1,0:T(8,128)(2,1)S(1)}, u32[]{:S(2)}, u32[]{:S(2)}) %collective-permute-start.1) | collective-permute-done | bytes 262176 | tf_op jit(solution)/shard_map/ppermute | solution.py:66
  20.0 5.7 %collective-permute-done.2 = bf16[256,512]{1,0:T(8,128)(2,1)S(1)} collective-permute-done((bf16[256,512]{1,0:T(8,128)(2,1)S(1)}, bf16[256,512]{1,0:T(8,128)(2,1)S(1)}, u32[]{:S(2)}, u32[]{:S(2)}) %collective-permute-start.2) | collective-permute-done | bytes 262176 | tf_op jit(solution)/shard_map/ppermute | solution.py:66
  27.6 24.9 %all-gather.6.cloned.1.call-done = bf16[2048,256]{1,0:T(8,128)(2,1)} async-done(((bf16[256,256]{1,0:T(8,128)(2,1)}), bf16[2048,256]{1,0:T(8,128)(2,1)}) %all-gather.6.cloned.1.call-update) | async-done | bytes 1048592 | tf_op jit(solution)/shard_map/all_gather | solution.py:85
  52.5 2.3 convolution_convert_fusion.1
  57.4 31.9 %all_gather.33 = bf16[2048,128]{1,0:T(8,128)(2,1)S(1)} all-gather(bf16[256,128]{1,0:T(8,128)(2,1)S(1)} %copy-done.5), channel_id=1, replica_groups=mesh['sp'=8,'tp'=4] {'sp'}, dimensions={0}, use_global_device_ids=true | all-gather | bytes 589824 | tf_op jit(solution)/shard_map/all_gather | solution.py:82
  89.2 31.9 %all_gather.35 = bf16[2048,128]{1,0:T(8,128)(2,1)S(1)} all-gather(bf16[256,128]{1,0:T(8,128)(2,1)S(1)} %copy-done.6), channel_id=1, replica_groups=mesh['sp'=8,'tp'=4] {'sp'}, dimensions={0}, use_global_device_ids=true | all-gather | bytes 589824 | tf_op jit(solution)/shard_map/all_gather | solution.py:81
  121.2 32.0 %all_gather.36 = bf16[2048,128]{1,0:T(8,128)(2,1)S(1)} all-gather(bf16[256,128]{1,0:T(8,128)(2,1)S(1)} %copy-done.7), channel_id=1, replica_groups=mesh['sp'=8,'tp'=4] {'sp'}, dimensions={0}, use_global_device_ids=true | all-gather | bytes 589824 | tf_op jit(solution)/shard_map/all_gather | solution.py:84
  153.2 32.3 %all_gather.38 = bf16[2048,128]{1,0:T(8,128)(2,1)S(1)} all-gather(bf16[256,128]{1,0:T(8,128)(2,1)S(1)} %copy-done.8), channel_id=1, replica_groups=mesh['sp'=8,'tp'=4] {'sp'}, dimensions={0}, use_global_device_ids=true | all-gather | bytes 589824 | tf_op jit(solution)/shard_map/all_gather | solution.py:83
  188.7 32.0 %all_gather.37 = bf16[2048,128]{0,1:T(8,128)(2,1)S(1)} all-gather(bf16[256,128]{0,1:T(8,128)(2,1)S(1)} %bitcast.251), channel_id=1, replica_groups=mesh['sp'=8,'tp'=4] {'sp'}, dimensions={0}, use_global_device_ids=true | all-gather | bytes 589824 | tf_op jit(solution)/shard_map/all_gather | solution.py:108
  220.8 31.5 %all_gather.34 = bf16[2048,128]{0,1:T(8,128)(2,1)S(1)} all-gather(bf16[256,128]{0,1:T(8,128)(2,1)S(1)} %bitcast.252), channel_id=1, replica_groups=mesh['sp'=8,'tp'=4] {'sp'}, dimensions={0}, use_global_device_ids=true | all-gather | bytes 589824 | tf_op jit(solution)/shard_map/all_gather | solution.py:107
  252.2 1.7 convolution_convert_fusion
  253.9 1.5 collective-permute-start.3
  258.2 1.3 reshape.313
  259.6 18.7 %while.15 = (s32[]{:T(128)}, f32[2,256,2]{1,2,0:T(2,128)S(1)}, f32[2,256,2]{1,2,0:T(2,128)S(1)}, f32[2,256,2,128]{1,3,2,0:T(8,128)S(1)}, s32[2]{0:T(128)S(1)}, /...) while((s32[]{:T(128)}, f32[2,256,2]{1,2,0:T(2,128)S(1)}, ...), condition=%wide.region_6.7_spmd.clone, body=%wide.region_1.6_spmd.clone.sunk | while | flops 416947456 | bytes 34822424 | solution.py:144
  261.2 1.9 fusion.141
  263.9 2.4 fusion.147
  266.3 1.0 fusion.143
  270.6 1.9 fusion.141
  273.2 2.4 fusion.147
  275.6 1.0 fusion.143
  278.7 1.7 fusion.101
  280.5 2.7 fusion.40
  283.2 25.4 %reduce-scatter.2.cloned.1.call-done = bf16[64,2048]{1,0:T(8,128)(2,1)} async-done(((bf16[256,2048]{1,0:T(8,128)(2,1)}), bf16[64,2048]{1,0:T(8,128)(2,1)}) %reduce-scatter.2.cloned.1.call-update) | async-done | bytes 262160 | tf_op jit(solution)/shard_map/reduce_scatter | solution.py:193
  (130 shorter events, 18.7 us)
Async XLA Ops:
  6.5 250.7 %copy-start = (bf16[8,128,128]{2,1,0:T(8,128)(2,1)S(1)}, bf16[8,128,128]{2,1,0:T(8,128)(2,1)}, u32[]{:S(2)}) copy-start(bf16[8,128,128]{2,1,0:T(8,128)(2,1)} %param.26) | copy-start | bytes 786436
  6.5 20.3 %copy-start.1 = (bf16[256,512]{1,0:T(8,128)(2,1)S(1)}, bf16[256,512]{1,0:T(8,128)(2,1)}, u32[]{:S(2)}) copy-start(bf16[256,512]{1,0:T(8,128)(2,1)} %param.16) | copy-start | bytes 786436
  6.5 46.0 %all-gather.6.cloned.1.call-start = ((), (), s32[]{:S(2)}) async-start(), calls=%async_computation.1 | async-start | bytes 1179648 | tf_op jit(solution)/shard_map/all_gather | solution.py:85
  7.3 245.0 %all-gather.12.cloned.1.call-start = ((), (), s32[]{:S(2)}) async-start(), calls=%async_computation.4 | async-start | bytes 1179648 | tf_op jit(solution)/shard_map/all_gather | solution.py:88
  7.3 6.8 %collective-permute-start = (bf16[256,512]{1,0:T(8,128)(2,1)}, bf16[256,512]{1,0:T(8,128)(2,1)S(1)}, u32[]{:S(2)}, u32[]{:S(2)}) collective-permute-start(bf16[256,512]{1,0:T(8,128)(2,1)} %param.16), channel_id=1, source_target_pairs={{0,1},{1,2},{2,3},{3,0},{4,5},{5,6},{6,7},{7,4},{8,9},{9,10},{10,1... | collective-permute-start | bytes 786440 | tf_op jit(solution)/shard_map/ppermute | solution.py:66
  14.1 5.8 %collective-permute-start.1 = (bf16[256,512]{1,0:T(8,128)(2,1)S(1)}, bf16[256,512]{1,0:T(8,128)(2,1)S(1)}, u32[]{:S(2)}, u32[]{:S(2)}) collective-permute-start(bf16[256,512]{1,0:T(8,128)(2,1)S(1)} %collective-permute-done), channel_id=1, source_target_pairs={{0,1},{1,2},{2,3},{3,0},{4,5},{5,6},{6,7},{7,4},{8,9},{9,10},{10,1... | collective-permute-start | bytes 786440 | tf_op jit(solution)/shard_map/ppermute | solution.py:66
  19.9 5.8 %collective-permute-start.2 = (bf16[256,512]{1,0:T(8,128)(2,1)S(1)}, bf16[256,512]{1,0:T(8,128)(2,1)S(1)}, u32[]{:S(2)}, u32[]{:S(2)}) collective-permute-start(bf16[256,512]{1,0:T(8,128)(2,1)S(1)} %collective-permute-done.1), channel_id=1, source_target_pairs={{0,1},{1,2},{2,3},{3,0},{4,5},{5,6},{6,7},{7,4},{8,9},{9,10},{10,1... | collective-permute-start | bytes 786440 | tf_op jit(solution)/shard_map/ppermute | solution.py:66
  19.9 238.3 %all-gather.8.cloned.1.call-start = ((), (), s32[]{:S(2)}) async-start(), calls=%async_computation.2 | async-start | bytes 1179648 | tf_op jit(solution)/shard_map/all_gather | solution.py:109
  27.2 30.2 %copy-start.5 = (bf16[256,128]{1,0:T(8,128)(2,1)S(1)}, bf16[256,128]{1,0:T(8,128)(2,1)}, u32[]{:S(2)}) copy-start(bf16[256,128]{1,0:T(8,128)(2,1)} %param.19) | copy-start | bytes 196612
  27.5 61.7 %copy-start.6 = (bf16[256,128]{1,0:T(8,128)(2,1)S(1)}, bf16[256,128]{1,0:T(8,128)(2,1)}, u32[]{:S(2)}) copy-start(bf16[256,128]{1,0:T(8,128)(2,1)} %param.18) | copy-start | bytes 196612
  27.5 93.6 %copy-start.7 = (bf16[256,128]{1,0:T(8,128)(2,1)S(1)}, bf16[256,128]{1,0:T(8,128)(2,1)}, u32[]{:S(2)}) copy-start(bf16[256,128]{1,0:T(8,128)(2,1)} %param.21) | copy-start | bytes 196612
  27.5 125.7 %copy-start.8 = (bf16[256,128]{1,0:T(8,128)(2,1)S(1)}, bf16[256,128]{1,0:T(8,128)(2,1)}, u32[]{:S(2)}) copy-start(bf16[256,128]{1,0:T(8,128)(2,1)} %param.20) | copy-start | bytes 196612
  27.6 158.9 %copy-start.11 = (f32[8]{0:T(128)S(1)}, f32[8]{0:T(128)}, u32[]{:S(2)}) copy-start(f32[8]{0:T(128)} %param.24) | copy-start | bytes 100
  27.6 159.0 %copy-start.10 = (f32[128]{0:T(128)S(1)}, f32[128]{0:T(128)}, u32[]{:S(2)}) copy-start(f32[128]{0:T(128)} %param.25) | copy-start | bytes 1540
  54.8 223.9 %all-gather.10.cloned.1.call-start = ((), (), s32[]{:S(2)}) async-start(), calls=%async_computation.3 | async-start | bytes 1179648 | tf_op jit(solution)/shard_map/all_gather | solution.py:190
  55.4 225.0 %all-gather.14.cloned.1.call-start = ((), (), s32[]{:S(2)}) async-start(), calls=%async_computation.5 | async-start | bytes 1179648 | tf_op jit(solution)/shard_map/all_gather | solution.py:191
  56.0 252.6 %reduce-scatter.2.cloned.1.call-start = ((), (), s32[]{:S(2)}) async-start(), calls=%async_computation.6 | async-start | bytes 1310720 | tf_op jit(solution)/shard_map/reduce_scatter | solution.py:193
  253.9 3.3 %collective-permute-start.3 = (bf16[15,256]{1,0:T(8,128)(2,1)S(1)}, bf16[15,256]{1,0:T(8,128)(2,1)S(1)}, u32[]{:S(2)}, u32[]{:S(2)}) collective-permute-start(bf16[15,256]{1,0:T(8,128)(2,1)S(1)} %slice.144), channel_id=1, source_target_pairs={{0,4},{4,8},{8,12},{12,16},{16,20},{20,24},{24,28},{1,5},{5,9},{9,... | collective-permute-start | bytes 23048 | tf_op jit(solution)/shard_map/ppermute | solution.py:22
  259.6 3.4 %copy-start.3 = (bf16[2,1024,2,64]{1,3,2,0:T(8,128)(2,1)}, bf16[2,1024,2,64]{1,3,2,0:T(8,128)(2,1)S(1)}, u32[]{:S(2)}) copy-start(bf16[2,1024,2,64]{1,3,2,0:T(8,128)(2,1)S(1)} %get-tuple-element.317) | copy-start | bytes 1572868 | tf_op jit(solution)/shard_map/while
  263.9 2.4 copy-start.2
  263.9 2.4 copy-start.12
  269.0 3.4 %copy-start.3 = (bf16[2,1024,2,64]{1,3,2,0:T(8,128)(2,1)}, bf16[2,1024,2,64]{1,3,2,0:T(8,128)(2,1)S(1)}, u32[]{:S(2)}) copy-start(bf16[2,1024,2,64]{1,3,2,0:T(8,128)(2,1)S(1)} %get-tuple-element.317) | copy-start | bytes 1572868 | tf_op jit(solution)/shard_map/while
  273.2 2.4 copy-start.2
  273.2 2.4 copy-start.12
  (5 other events, 7.3 us)
Sparse Core Ops, SparseCore 0:
  9.5 42.9 all-gather.5
  54.6 41.8 all-gather.11
  98.7 41.9 all-gather.7
  142.5 41.8 all-gather.9
  186.3 40.4 all-gather.13
  283.3 25.2 reduce-scatter.1
